TPU v7x, 256 devices: a 8x8x2 block of a 8x8x16 slice. The times are simulated.
256 devices in a mesh: grp: 2 (over z), fs: 16 (over y, core), tp: 8 (over x).
Axes of the slice: x: 8, y: 8, z: 2, core: 2. Of those that a mesh axis runs over, the one named last changes fastest.
The devices are a block of a 8x8x16 slice.
Arguments:
- stream: bfloat16 [32768, 2048], P(('grp', 'fs', 'tp')), parts along dimension 0, may hold values from -4 to 4
- gain_first: bfloat16 [2048], replicated, may hold values from 0.099609375 to 1.8984375
- gate_first: bfloat16 [2048, 4096], P('fs', 'tp'), may hold values from -0.125 to 0.125
- up_first: bfloat16 [2048, 4096], P('fs', 'tp'), may hold values from -0.125 to 0.125
- down_first: bfloat16 [4096, 2048], P('tp', 'fs'), may hold values from -0.09375 to 0.09375
- gain_second: bfloat16 [2048], replicated, may hold values from 0.099609375 to 1.8984375
- gate_second: bfloat16 [2048, 4096], P('fs', 'tp'), may hold values from -0.125 to 0.125
- up_second: bfloat16 [2048, 4096], P('fs', 'tp'), may hold values from -0.125 to 0.125
- down_second: bfloat16 [4096, 2048], P('tp', 'fs'), may hold values from -0.09375 to 0.09375
Outputs:
- result: bfloat16 [32768, 2048], P(('grp', 'fs', 'tp')), parts along dimension 0
There are 2 independent parts, one for each index of `grp`. A program takes and returns all parts, laid end to end along the dimension named above; an argument that names none is the same for every part. Nothing has to cross between parts.
All inputs are finite; a program needn't handle non-finite values.
Results may differ from a plain program's by a relative error of at most 0.018.
Values may be sent and summed in bfloat16 or wider, within the bound.
A program may use at most 64 MiB of HBM per device.

v0:
```python
import jax
import jax.numpy as jnp
from jax import lax
from jax.sharding import PartitionSpec as P


def gather_turned(arrays, axis, dims):
    turned = [jnp.moveaxis(a, dim, 0) for a, dim in zip(arrays, dims)]
    widths = [t[0].size for t in turned]
    both = jnp.concatenate([t.reshape(-1, w) for t, w in zip(turned, widths)], axis=1)
    result = lax.all_gather(both, axis, axis=0, tiled=True)
    blocks = jnp.split(result, [sum(widths[:k]) for k in range(1, len(widths))], axis=1)
    return tuple(
        (
            jnp.moveaxis(b.reshape(-1, *t.shape[1:]), 0, dim)
            for b, t, dim in zip(blocks, turned, dims)
        )
    )


def half_branch(stream, gain, gathered):
    stream_f = stream.astype(jnp.float32)
    normed = (
        stream_f
        * lax.rsqrt(jnp.mean(stream_f * stream_f, axis=-1, keepdims=True) + 1e-06)
        * gain.astype(jnp.float32)
    ).astype(jnp.bfloat16)
    tokens = lax.all_gather(normed, "tp", axis=0, tiled=True)
    gate_act = jnp.dot(tokens, gathered[0], preferred_element_type=jnp.float32)
    up_act = jnp.dot(tokens, gathered[1], preferred_element_type=jnp.float32)
    down_full = gathered[2]
    hidden = (jax.nn.silu(gate_act) * up_act).astype(jnp.bfloat16)
    summed = lax.psum_scatter(
        jnp.dot(hidden, down_full, preferred_element_type=jnp.float32).astype(jnp.bfloat16),
        "tp",
        scatter_dimension=0,
        tiled=True,
    ).astype(jnp.float32)
    return (stream_f + 0.5 * summed).astype(jnp.bfloat16)


def local(
    stream,
    gain_first,
    gate_first,
    up_first,
    down_first,
    gain_second,
    gate_second,
    up_second,
    down_second,
):
    weights = gather_turned(
        (gate_first, up_first, down_first, gate_second, up_second, down_second),
        "fs",
        (0, 0, 1, 0, 0, 1),
    )
    first_set = (weights[0], weights[1], weights[2])
    second_set = (weights[3], weights[4], weights[5])
    middle = half_branch(stream, gain_first, first_set)
    return half_branch(middle, gain_second, second_set)


def solution(mesh):
    in_specs = (
        P(("grp", "fs", "tp"), None),
        P(),
        P("fs", "tp"),
        P("fs", "tp"),
        P("tp", "fs"),
        P(),
        P("fs", "tp"),
        P("fs", "tp"),
        P("tp", "fs"),
    )
    out_specs = P(("grp", "fs", "tp"), None)
    return jax.shard_map(local, mesh=mesh, in_specs=in_specs, out_specs=out_specs, check_vma=False)
```

profile of v0, /device:TPU:513, one launch (start us, length us, event | category | flops | bytes accessed | tf_op | source)
XLA Modules:
  0.0 377.2 jit_solution(9833353432578024981)
XLA Ops:
  6.6 1.3 fusion.18
  8.0 0.7 convert_element_type.43
  8.7 2.0 fusion.20
  10.8 0.1 all-gather.6.cloned.1.call-start
  10.9 0.1 copy.10
  11.0 0.1 copy.11
  11.2 0.1 copy.12
  11.3 0.1 copy.13
  11.6 0.9 copy-done.2
  12.5 0.1 reduce-scatter.3.cloned.1.call-start
  12.6 72.6 %all-gather.4.cloned.1.call-done = bf16[1024,2048]{1,0:T(8,128)(2,1)} async-done(((bf16[128,2048]{1,0:T(8,128)(2,1)}), bf16[1024,2048]{1,0:T(8,128)(2,1)}) %all-gather.4.cloned.1.call-update) | async-done | bytes 4194320 | tf_op jit(solution)/shard_map/all_gather | solution.py:28
  85.2 84.5 %all-gather.6.cloned.1.call-done = bf16[2048,3072]{0,1:T(8,128)(2,1)} async-done(((bf16[128,3072]{0,1:T(8,128)(2,1)}), bf16[2048,3072]{0,1:T(8,128)(2,1)}) %all-gather.6.cloned.1.call-update) | async-done | bytes 12582928 | tf_op jit(solution)/shard_map/all_gather | solution.py:11
  169.7 5.2 %fusion.8 = f32[1024,512]{1,0:T(8,128)S(1)} fusion(bf16[1024,2048]{1,0:T(8,128)(2,1)} %all-gather.4.cloned.1.call-done, bf16[2048,3072]{0,1:T(8,128)(2,1)} %all-gather.6.cloned.1.call-done), kind=kOutput, calls=%fused_computation.10 | convolution fusion | flops 2147483648 | bytes 8388608 | tf_op jit(solution)/shard_map/dot_general | solution.py:29
  174.9 10.0 %convolution_convert_fusion.1 = bf16[1024,2048]{1,0:T(8,128)(2,1)} fusion(bf16[2048,3072]{0,1:T(8,128)(2,1)} %all-gather.6.cloned.1.call-done, f32[1024,512]{1,0:T(8,128)S(1)} %fusion.8, bf16[1024,2048]{1,0:T(8,128)(2,1)} %all-gather.4.cloned.1.call-done), kind=kOutput, calls=%fused_computation.1 | convolution fusion | flops 4300210176 | bytes 14680064 | tf_op jit(solution)/shard_map/dot_general | solution.py:34
  185.1 0.5 copy-done.9
  185.6 53.6 %reduce-scatter.3.cloned.1.call-done = bf16[128,2048]{1,0:T(8,128)(2,1)} async-done(((bf16[1024,2048]{1,0:T(8,128)(2,1)}), bf16[128,2048]{1,0:T(8,128)(2,1)}) %reduce-scatter.3.cloned.1.call-update) | async-done | bytes 524304 | tf_op jit(solution)/shard_map/reduce_scatter | solution.py:33
  239.2 1.3 fusion.22
  240.6 2.1 fusion.24
  242.7 0.2 reduce-scatter.5.cloned.1.call-start
  243.0 54.6 %all-gather.8.cloned.1.call-done = bf16[1024,2048]{1,0:T(8,128)(2,1)} async-done(((bf16[128,2048]{1,0:T(8,128)(2,1)}), bf16[1024,2048]{1,0:T(8,128)(2,1)}) %all-gather.8.cloned.1.call-update) | async-done | bytes 4194320 | tf_op jit(solution)/shard_map/all_gather | solution.py:28
  297.6 5.2 %fusion.3 = f32[1024,512]{1,0:T(8,128)S(1)} fusion(bf16[1024,2048]{1,0:T(8,128)(2,1)} %all-gather.8.cloned.1.call-done, bf16[2048,3072]{0,1:T(8,128)(2,1)} %all-gather.6.cloned.1.call-done), kind=kOutput, calls=%fused_computation.5 | convolution fusion | flops 2147483648 | bytes 8388608 | tf_op jit(solution)/shard_map/dot_general | solution.py:29
  302.8 10.0 %convolution_convert_fusion = bf16[1024,2048]{1,0:T(8,128)(2,1)} fusion(bf16[2048,3072]{0,1:T(8,128)(2,1)} %all-gather.6.cloned.1.call-done, f32[1024,512]{1,0:T(8,128)S(1)} %fusion.3, bf16[1024,2048]{1,0:T(8,128)(2,1)} %all-gather.8.cloned.1.call-done), kind=kOutput, calls=%fused_computation | convolution fusion | flops 4300210176 | bytes 14680064 | tf_op jit(solution)/shard_map/dot_general | solution.py:34
  312.9 55.6 %reduce-scatter.5.cloned.1.call-done = bf16[128,2048]{1,0:T(8,128)(2,1)} async-done(((bf16[1024,2048]{1,0:T(8,128)(2,1)}), bf16[128,2048]{1,0:T(8,128)(2,1)}) %reduce-scatter.5.cloned.1.call-update) | async-done | bytes 524304 | tf_op jit(solution)/shard_map/reduce_scatter | solution.py:33
  368.5 2.1 fusion.25
  (34 shorter events, 0.6 us)
Async XLA Ops:
  6.5 4.3 %copy-start.3 = (bf16[128,512]{1,0:T(8,128)(2,1)S(1)}, bf16[128,512]{1,0:T(8,128)(2,1)}, u32[]{:S(2)}) copy-start(bf16[128,512]{1,0:T(8,128)(2,1)} %param.11) | copy-start | bytes 393220
  6.5 4.5 %copy-start.4 = (bf16[128,512]{1,0:T(8,128)(2,1)S(1)}, bf16[128,512]{1,0:T(8,128)(2,1)}, u32[]{:S(2)}) copy-start(bf16[128,512]{1,0:T(8,128)(2,1)} %param.12) | copy-start | bytes 393220
  6.6 4.6 %copy-start.5 = (bf16[128,512]{1,0:T(8,128)(2,1)S(1)}, bf16[128,512]{1,0:T(8,128)(2,1)}, u32[]{:S(2)}) copy-start(bf16[128,512]{1,0:T(8,128)(2,1)} %param.15) | copy-start | bytes 393220
  6.6 4.7 %copy-start.6 = (bf16[128,512]{1,0:T(8,128)(2,1)S(1)}, bf16[128,512]{1,0:T(8,128)(2,1)}, u32[]{:S(2)}) copy-start(bf16[128,512]{1,0:T(8,128)(2,1)} %param.16) | copy-start | bytes 393220
  6.6 4.9 %copy-start.7 = (bf16[512,128]{1,0:T(8,128)(2,1)S(1)}, bf16[512,128]{1,0:T(8,128)(2,1)}, u32[]{:S(2)}) copy-start(bf16[512,128]{1,0:T(8,128)(2,1)} %param.13) | copy-start | bytes 393220
  6.6 78.6 %all-gather.4.cloned.1.call-start = ((), (), s32[]{:S(2)}) async-start(), calls=%async_computation.2 | async-start | bytes 4718592 | tf_op jit(solution)/shard_map/all_gather | solution.py:28
  8.0 3.6 copy-start.8
  10.8 158.9 %all-gather.6.cloned.1.call-start = ((), (), s32[]{:S(2)}) async-start(), calls=%async_computation.3 | async-start | bytes 13369344 | tf_op jit(solution)/shard_map/all_gather | solution.py:11
  11.6 0.9 copy-start.2
  12.5 226.7 %reduce-scatter.3.cloned.1.call-start = ((), (), s32[]{:S(2)}) async-start(), calls=%async_computation.4 | async-start | bytes 4718592 | tf_op jit(solution)/shard_map/reduce_scatter | solution.py:33
  185.0 0.7 copy-start.9
  185.0 54.3 %copy-start = (bf16[128,2048]{1,0:T(8,128)(2,1)S(1)}, bf16[128,2048]{1,0:T(8,128)(2,1)}, u32[]{:S(2)}) copy-start(bf16[128,2048]{1,0:T(8,128)(2,1)} %param.9) | copy-start | bytes 1572868
  185.0 112.6 %all-gather.8.cloned.1.call-start = ((), (), s32[]{:S(2)}) async-start(), calls=%async_computation.5 | async-start | bytes 4718592 | tf_op jit(solution)/shard_map/all_gather | solution.py:28
  242.7 125.8 %reduce-scatter.5.cloned.1.call-start = ((), (), s32[]{:S(2)}) async-start(), calls=%async_computation.6 | async-start | bytes 4718592 | tf_op jit(solution)/shard_map/reduce_scatter | solution.py:33
  312.8 55.7 %copy-start.1 = (bf16[128,2048]{1,0:T(8,128)(2,1)S(1)}, bf16[128,2048]{1,0:T(8,128)(2,1)}, u32[]{:S(2)}) copy-start(bf16[128,2048]{1,0:T(8,128)(2,1)} %reduce-scatter.3.cloned.1.call-done) | copy-start | bytes 1572868
Sparse Core Ops, SparseCore 0:
  10.9 74.2 all-gather.3
  86.9 82.7 all-gather.5
  185.1 54.0 reduce-scatter.2
  242.8 54.7 all-gather.7
  313.0 55.4 reduce-scatter.4
where the time goes:
time: 377 us
  waiting for transfers between devices  321 us (85%)
  matrix products  30.5 us (8%)
  between operations  13.3 us (4%)
  other arithmetic  9.61 us (3%)
    all_gather x2, waiting for transfers between devices, half_branch(): tokens = lax.all_gather(normed, 'tp', axis=0, tiled=True)  127 us
    reduce_scatter x2, waiting for transfers between devices, half_branch(): lax.psum_scatter(jnp.dot(hidden, down_full, preferred_element_type=jnp.fl...  109 us
    all_gather x1, waiting for transfers between devices, gather_turned(): result = lax.all_gather(both, axis, axis=0, tiled=True)  84.5 us
    dot_general x2, matrix products, half_branch(): jnp.dot(hidden, down_full, preferred_element_type=jnp.float32)  20 us
    dot_general x2, matrix products, half_branch(): gate_act = jnp.dot(tokens, gathered[0], preferred_element_type=jnp.float32)  10.4 us
  transfers between devices with their start and end apart: 5, of which 5 were waited for; matrix products, arithmetic and copies ran while one was open for 0% of the time, Pallas kernels for 0%

commit v1 on v0

--- a/solution.py
+++ b/solution.py
@@ -1,7 +1,38 @@
+import functools
 import jax
 import jax.numpy as jnp
 from jax import lax
 from jax.sharding import PartitionSpec as P
+
+
+def _work_space(sample, join_dim, mesh_dim):
+    vec_out, part_now, k_now = (
+        lax.axis_size(mesh_dim),
+        lax.axis_index(mesh_dim),
+        sample.shape[join_dim],
+    )
+    pages = [(src_i, (src_i + 1) % vec_out) for src_i in range(vec_out)]
+    all_blocks = [(src_i, (src_i - 1) % vec_out) for src_i in range(vec_out)]
+    x_now = jnp.zeros(
+        (*sample.shape[:join_dim], vec_out * k_now, *sample.shape[join_dim + 1 :]), sample.dtype
+    )
+    x_now = lax.dynamic_update_slice_in_dim(x_now, sample, part_now * k_now, axis=join_dim)
+    u1 = main = sample
+    then = vec_out // 2
+    for dd in range(1, then + 1):
+        u1 = lax.ppermute(u1, mesh_dim, pages)
+        x_now = lax.dynamic_update_slice_in_dim(
+            x_now, u1, (part_now - dd) % vec_out * k_now, axis=join_dim
+        )
+        if dd < vec_out - then:
+            main = lax.ppermute(main, mesh_dim, all_blocks)
+            x_now = lax.dynamic_update_slice_in_dim(
+                x_now, main, (part_now + dd) % vec_out * k_now, axis=join_dim
+            )
+    return x_now
+
+
+_link_rails = functools.partial(_work_space, join_dim=0, mesh_dim="tp")
 
 
 def gather_turned(arrays, axis, dims):
@@ -25,7 +56,7 @@
         * lax.rsqrt(jnp.mean(stream_f * stream_f, axis=-1, keepdims=True) + 1e-06)
         * gain.astype(jnp.float32)
     ).astype(jnp.bfloat16)
-    tokens = lax.all_gather(normed, "tp", axis=0, tiled=True)
+    tokens = _link_rails(normed)
     gate_act = jnp.dot(tokens, gathered[0], preferred_element_type=jnp.float32)
     up_act = jnp.dot(tokens, gathered[1], preferred_element_type=jnp.float32)
     down_full = gathered[2]

time: 377 us -> 327 us (0.87)
  waiting for transfers between devices: 321 us -> 232 us
  starting transfers between devices: 0.5 us -> 21.7 us
  local copies, waits for them, and re-layouts: 2.05 us -> 18.7 us
    all_gather x2 -> x0, waiting for transfers between devices: 127 us -> none  [half_branch(): tokens = lax.all_gather(normed, 'tp', axis=0, tiled=True)]
    ppermute x0 -> x14, waiting for transfers between devices: none -> 73 us  [the longest x8 73 us: _work_space(): u1 = lax.ppermute(u1, mesh_dim, pages)]
    all_gather x1, waiting for transfers between devices: 84.5 us -> 46.7 us  [gather_turned(): result = lax.all_gather(both, axis, axis=0, tiled=True)]
    ppermute x0 -> x14, starting transfers between devices: none -> 21.6 us  [the longest x6 16 us: _work_space(): main = lax.ppermute(main, mesh_dim, all_blocks)]
    unnamed x29 -> x19, local copies, waits for them, and re-layouts: 2.03 us -> 8.6 us
    dynamic_update_slice x0 -> x14, local copies, waits for them, and re-layouts: none -> 6.22 us  [the longest x8 3.54 us: _work_space(): lax.dynamic_update_slice_in_dim(x_now, u1, (part_now - dd) % vec_out * k_...]
    convert_element_type x2 -> x0, other arithmetic: 4.09 us -> none  [half_branch(): normed = (stream_f * lax.rsqrt(jnp.mean(stream_f * stream_f, axis=-1, kee...]
  transfers between devices with their start and end apart: 5 -> 17, of which waited for: 5 -> 11; matrix products, arithmetic and copies ran while one was open for 0% -> 4% of each run, Pallas kernels for 0% -> 0%
where the time goes in v1:
time: 327 us; the launch traced here: 326 us
  waiting for transfers between devices  232 us (71%)
  matrix products  33.3 us (10%)
  starting transfers between devices  21.7 us (7%)
  local copies, waits for them, and re-layouts  18.7 us (6%)
  between operations  13.3 us (4%)
  other arithmetic  6.7 us (2%)
    reduce_scatter x2, waiting for transfers between devices, half_branch(): lax.psum_scatter(jnp.dot(hidden, down_full, preferred_element_type=jnp.fl...  113 us
    ppermute x8, waiting for transfers between devices, _work_space(): u1 = lax.ppermute(u1, mesh_dim, pages)  73 us
    all_gather x1, waiting for transfers between devices, gather_turned(): result = lax.all_gather(both, axis, axis=0, tiled=True)  46.7 us
    dot_general x2, matrix products, half_branch(): jnp.dot(hidden, down_full, preferred_element_type=jnp.float32)  21.4 us
    ppermute x6, starting transfers between devices, _work_space(): main = lax.ppermute(main, mesh_dim, all_blocks)  16 us
    dot_general x2, matrix products, half_branch(): up_act = jnp.dot(tokens, gathered[1], preferred_element_type=jnp.float32)  11.9 us
    unnamed x19, local copies, waits for them, and re-layouts  8.6 us
  transfers between devices with their start and end apart: 17, of which 11 were waited for; matrix products, arithmetic and copies ran while one was open for 4% of the time, Pallas kernels for 0%

profile of v1, /device:TPU:513, one launch (start us, length us, event | category | flops | bytes accessed | tf_op | source)
XLA Modules:
  0.0 326.3 jit_solution(5056681049691570151)
XLA Ops:
  15.7 2.5 broadcast.46.clone
  19.2 2.2 collective-permute-start
  21.3 2.2 collective-permute-start.1
  23.5 6.6 %collective-permute-done = bf16[128,2048]{1,0:T(8,128)(2,1)S(1)} collective-permute-done((bf16[128,2048]{1,0:T(8,128)(2,1)S(1)}, bf16[128,2048]{1,0:T(8,128)(2,1)S(1)}, u32[]{:S(2)}, u32[]{:S(2)}) %collective-permute-start) | collective-permute-done | bytes 524320 | tf_op jit(solution)/shard_map/ppermute | solution.py:23
  30.1 3.3 %collective-permute-start.2 = (bf16[128,2048]{1,0:T(8,128)(2,1)S(1)}, bf16[128,2048]{1,0:T(8,128)(2,1)S(1)}, u32[]{:S(2)}, u32[]{:S(2)}) collective-permute-start(bf16[128,2048]{1,0:T(8,128)(2,1)S(1)} %collective-permute-done), channel_id=1, source_target_pairs={{0,1},{1,2},{2,3},{3,4},{4,5},{5,6},{6,7},{7,0},{8,9},{9,10},{10,1... | collective-permute-start | bytes 1572872 | tf_op jit(solution)/shard_map/ppermute | solution.py:23
  33.4 3.0 collective-permute-start.3
  36.4 6.6 %collective-permute-done.2 = bf16[128,2048]{1,0:T(8,128)(2,1)S(1)} collective-permute-done((bf16[128,2048]{1,0:T(8,128)(2,1)S(1)}, bf16[128,2048]{1,0:T(8,128)(2,1)S(1)}, u32[]{:S(2)}, u32[]{:S(2)}) %collective-permute-start.2) | collective-permute-done | bytes 524320 | tf_op jit(solution)/shard_map/ppermute | solution.py:23
  44.7 2.7 collective-permute-start.5
  48.2 7.2 %collective-permute-done.4 = bf16[128,2048]{1,0:T(8,128)(2,1)S(1)} collective-permute-done((bf16[128,2048]{1,0:T(8,128)(2,1)S(1)}, bf16[128,2048]{1,0:T(8,128)(2,1)S(1)}, u32[]{:S(2)}, u32[]{:S(2)}) %collective-permute-start.4) | collective-permute-done | bytes 524320 | tf_op jit(solution)/shard_map/ppermute | solution.py:23
  57.9 10.5 %collective-permute-done.6 = bf16[128,2048]{1,0:T(8,128)(2,1)S(1)} collective-permute-done((bf16[128,2048]{1,0:T(8,128)(2,1)S(1)}, bf16[128,2048]{1,0:T(8,128)(2,1)S(1)}, u32[]{:S(2)}, u32[]{:S(2)}) %collective-permute-start.6) | collective-permute-done | bytes 524320 | tf_op jit(solution)/shard_map/ppermute | solution.py:23
  69.3 46.7 %all-gather.2.cloned.1.call-done = bf16[2048,3072]{0,1:T(8,128)(2,1)} async-done(((bf16[128,3072]{0,1:T(8,128)(2,1)}), bf16[2048,3072]{0,1:T(8,128)(2,1)}) %all-gather.2.cloned.1.call-update) | async-done | bytes 12582928 | tf_op jit(solution)/shard_map/all_gather | solution.py:42
  116.0 6.6 %fusion.6 = f32[1024,512]{1,0:T(8,128)} fusion(bf16[1024,2048]{1,0:T(8,128)(2,1)} %constant_dynamic-update-slice_fusion.12, bf16[2048,3072]{0,1:T(8,128)(2,1)} %all-gather.2.cloned.1.call-done), kind=kOutput, calls=%fused_computation.8 | convolution fusion | flops 2147483648 | bytes 8388608 | tf_op jit(solution)/shard_map/dot_general | solution.py:61
  122.6 10.7 %convolution_convert_fusion.1 = bf16[1024,2048]{1,0:T(8,128)(2,1)} fusion(bf16[2048,3072]{0,1:T(8,128)(2,1)} %all-gather.2.cloned.1.call-done, f32[1024,512]{1,0:T(8,128)} %fusion.6, bf16[1024,2048]{1,0:T(8,128)(2,1)} %constant_dynamic-update-slice_fusion.12), kind=kOutput, calls=%fused_computation.1 | convolution fusion | flops 4300210176 | bytes 14680064 | tf_op jit(solution)/shard_map/dot_general | solution.py:65
  134.0 53.6 %reduce-scatter.3.cloned.1.call-done = bf16[128,2048]{1,0:T(8,128)(2,1)} async-done(((bf16[1024,2048]{1,0:T(8,128)(2,1)}), bf16[128,2048]{1,0:T(8,128)(2,1)}) %reduce-scatter.3.cloned.1.call-update) | async-done | bytes 524304 | tf_op jit(solution)/shard_map/reduce_scatter | solution.py:64
  189.9 2.6 collective-permute-start.8
  192.6 11.3 %collective-permute-done.7 = bf16[128,2048]{1,0:T(8,128)(2,1)S(1)} collective-permute-done((bf16[128,2048]{1,0:T(8,128)(2,1)S(1)}, bf16[128,2048]{1,0:T(8,128)(2,1)S(1)}, u32[]{:S(2)}, u32[]{:S(2)}) %collective-permute-start.7) | collective-permute-done | bytes 524320 | tf_op jit(solution)/shard_map/ppermute | solution.py:23
  203.8 2.7 collective-permute-start.10
  206.5 10.4 %collective-permute-done.9 = bf16[128,2048]{1,0:T(8,128)(2,1)S(1)} collective-permute-done((bf16[128,2048]{1,0:T(8,128)(2,1)S(1)}, bf16[128,2048]{1,0:T(8,128)(2,1)S(1)}, u32[]{:S(2)}, u32[]{:S(2)}) %collective-permute-start.9) | collective-permute-done | bytes 524320 | tf_op jit(solution)/shard_map/ppermute | solution.py:23
  217.1 2.8 collective-permute-start.12
  219.9 9.3 %collective-permute-done.11 = bf16[128,2048]{1,0:T(8,128)(2,1)S(1)} collective-permute-done((bf16[128,2048]{1,0:T(8,128)(2,1)S(1)}, bf16[128,2048]{1,0:T(8,128)(2,1)S(1)}, u32[]{:S(2)}, u32[]{:S(2)}) %collective-permute-start.11) | collective-permute-done | bytes 524320 | tf_op jit(solution)/shard_map/ppermute | solution.py:23
  229.4 11.2 %collective-permute-done.13 = bf16[128,2048]{1,0:T(8,128)(2,1)S(1)} collective-permute-done((bf16[128,2048]{1,0:T(8,128)(2,1)S(1)}, bf16[128,2048]{1,0:T(8,128)(2,1)S(1)}, u32[]{:S(2)}, u32[]{:S(2)}) %collective-permute-start.13) | collective-permute-done | bytes 524320 | tf_op jit(solution)/shard_map/ppermute | solution.py:23
  242.6 5.3 %fusion.1 = f32[1024,512]{1,0:T(8,128)} fusion(bf16[1024,2048]{1,0:T(8,128)(2,1)S(1)} %constant_dynamic-update-slice_fusion.4, bf16[2048,3072]{0,1:T(8,128)(2,1)} %all-gather.2.cloned.1.call-done), kind=kOutput, calls=%fused_computation.3 | convolution fusion | flops 2147483648 | bytes 8388608 | tf_op jit(solution)/shard_map/dot_general | solution.py:61
  247.9 10.7 %convolution_convert_fusion = bf16[1024,2048]{1,0:T(8,128)(2,1)} fusion(bf16[2048,3072]{0,1:T(8,128)(2,1)} %all-gather.2.cloned.1.call-done, f32[1024,512]{1,0:T(8,128)} %fusion.1, bf16[1024,2048]{1,0:T(8,128)(2,1)} %copy-done.2), kind=kOutput, calls=%fused_computation | convolution fusion | flops 4300210176 | bytes 14680064 | tf_op jit(solution)/shard_map/dot_general | solution.py:65
  258.6 59.0 %reduce-scatter.5.cloned.1.call-done = bf16[128,2048]{1,0:T(8,128)(2,1)} async-done(((bf16[1024,2048]{1,0:T(8,128)(2,1)}), bf16[128,2048]{1,0:T(8,128)(2,1)}) %reduce-scatter.5.cloned.1.call-update) | async-done | bytes 524304 | tf_op jit(solution)/shard_map/reduce_scatter | solution.py:64
  (62 shorter events, 23.4 us)
Async XLA Ops:
  6.5 11.6 %copy-start = (bf16[128,2048]{1,0:T(8,128)(2,1)S(1)}, bf16[128,2048]{1,0:T(8,128)(2,1)}, u32[]{:S(2)}) copy-start(bf16[128,2048]{1,0:T(8,128)(2,1)} %param.9) | copy-start | bytes 1572868
  6.5 109.4 %all-gather.2.cloned.1.call-start = ((), (), s32[]{:S(2)}) async-start(), calls=%async_computation.2 | async-start | bytes 13369344 | tf_op jit(solution)/shard_map/all_gather | solution.py:42
  12.7 1.0 copy-start.3
  13.7 173.8 %reduce-scatter.3.cloned.1.call-start = ((), (), s32[]{:S(2)}) async-start(), calls=%async_computation.3 | async-start | bytes 4718592 | tf_op jit(solution)/shard_map/reduce_scatter | solution.py:64
  19.2 10.9 %collective-permute-start = (bf16[128,2048]{1,0:T(8,128)(2,1)S(1)}, bf16[128,2048]{1,0:T(8,128)(2,1)S(1)}, u32[]{:S(2)}, u32[]{:S(2)}) collective-permute-start(bf16[128,2048]{1,0:T(8,128)(2,1)S(1)} %get-tuple-element.8), channel_id=1, source_target_pairs={{0,1},{1,2},{2,3},{3,4},{4,5},{5,6},{6,7},{7,0},{8,9},{9,10},{10,1... | collective-permute-start | bytes 1572872 | tf_op jit(solution)/shard_map/ppermute | solution.py:23
  21.3 12.0 %collective-permute-start.1 = (bf16[128,2048]{1,0:T(8,128)(2,1)S(1)}, bf16[128,2048]{1,0:T(8,128)(2,1)S(1)}, u32[]{:S(2)}, u32[]{:S(2)}) collective-permute-start(bf16[128,2048]{1,0:T(8,128)(2,1)S(1)} %get-tuple-element.8), channel_id=1, source_target_pairs={{0,7},{1,0},{2,1},{3,2},{4,3},{5,4},{6,5},{7,6},{8,15},{9,8},{10,9... | collective-permute-start | bytes 1572872 | tf_op jit(solution)/shard_map/ppermute | solution.py:28
  30.1 12.9 %collective-permute-start.2 = (bf16[128,2048]{1,0:T(8,128)(2,1)S(1)}, bf16[128,2048]{1,0:T(8,128)(2,1)S(1)}, u32[]{:S(2)}, u32[]{:S(2)}) collective-permute-start(bf16[128,2048]{1,0:T(8,128)(2,1)S(1)} %collective-permute-done), channel_id=1, source_target_pairs={{0,1},{1,2},{2,3},{3,4},{4,5},{5,6},{6,7},{7,0},{8,9},{9,10},{10,1... | collective-permute-start | bytes 1572872 | tf_op jit(solution)/shard_map/ppermute | solution.py:23
  33.4 11.3 %collective-permute-start.3 = (bf16[128,2048]{1,0:T(8,128)(2,1)S(1)}, bf16[128,2048]{1,0:T(8,128)(2,1)S(1)}, u32[]{:S(2)}, u32[]{:S(2)}) collective-permute-start(bf16[128,2048]{1,0:T(8,128)(2,1)S(1)} %collective-permute-done.1), channel_id=1, source_target_pairs={{0,7},{1,0},{2,1},{3,2},{4,3},{5,4},{6,5},{7,6},{8,15},{9,8},{10,9... | collective-permute-start | bytes 1572872 | tf_op jit(solution)/shard_map/ppermute | solution.py:28
  43.0 12.3 %collective-permute-start.4 = (bf16[128,2048]{1,0:T(8,128)(2,1)S(1)}, bf16[128,2048]{1,0:T(8,128)(2,1)S(1)}, u32[]{:S(2)}, u32[]{:S(2)}) collective-permute-start(bf16[128,2048]{1,0:T(8,128)(2,1)S(1)} %collective-permute-done.2), channel_id=1, source_target_pairs={{0,1},{1,2},{2,3},{3,4},{4,5},{5,6},{6,7},{7,0},{8,9},{9,10},{10,1... | collective-permute-start | bytes 1572872 | tf_op jit(solution)/shard_map/ppermute | solution.py:23
  44.7 12.4 %collective-permute-start.5 = (bf16[128,2048]{1,0:T(8,128)(2,1)S(1)}, bf16[128,2048]{1,0:T(8,128)(2,1)S(1)}, u32[]{:S(2)}, u32[]{:S(2)}) collective-permute-start(bf16[128,2048]{1,0:T(8,128)(2,1)S(1)} %collective-permute-done.3), channel_id=1, source_target_pairs={{0,7},{1,0},{2,1},{3,2},{4,3},{5,4},{6,5},{7,6},{8,15},{9,8},{10,9... | collective-permute-start | bytes 1572872 | tf_op jit(solution)/shard_map/ppermute | solution.py:28
  55.3 13.1 %collective-permute-start.6 = (bf16[128,2048]{1,0:T(8,128)(2,1)S(1)}, bf16[128,2048]{1,0:T(8,128)(2,1)S(1)}, u32[]{:S(2)}, u32[]{:S(2)}) collective-permute-start(bf16[128,2048]{1,0:T(8,128)(2,1)S(1)} %collective-permute-done.4), channel_id=1, source_target_pairs={{0,1},{1,2},{2,3},{3,4},{4,5},{5,6},{6,7},{7,0},{8,9},{9,10},{10,1... | collective-permute-start | bytes 1572872 | tf_op jit(solution)/shard_map/ppermute | solution.py:23
  133.3 0.7 copy-start.4
  133.3 184.3 %reduce-scatter.5.cloned.1.call-start = ((), (), s32[]{:S(2)}) async-start(), calls=%async_computation.4 | async-start | bytes 4718592 | tf_op jit(solution)/shard_map/reduce_scatter | solution.py:64
  187.5 1.9 copy-start.1
  189.8 14.1 %collective-permute-start.7 = (bf16[128,2048]{1,0:T(8,128)(2,1)S(1)}, bf16[128,2048]{1,0:T(8,128)(2,1)S(1)}, u32[]{:S(2)}, u32[]{:S(2)}) collective-permute-start(bf16[128,2048]{1,0:T(8,128)(2,1)S(1)} %get-tuple-element.6), channel_id=1, source_target_pairs={{0,1},{1,2},{2,3},{3,4},{4,5},{5,6},{6,7},{7,0},{8,9},{9,10},{10,1... | collective-permute-start | bytes 1572872 | tf_op jit(solution)/shard_map/ppermute | solution.py:23
  189.9 13.9 %collective-permute-start.8 = (bf16[128,2048]{1,0:T(8,128)(2,1)S(1)}, bf16[128,2048]{1,0:T(8,128)(2,1)S(1)}, u32[]{:S(2)}, u32[]{:S(2)}) collective-permute-start(bf16[128,2048]{1,0:T(8,128)(2,1)S(1)} %get-tuple-element.6), channel_id=1, source_target_pairs={{0,7},{1,0},{2,1},{3,2},{4,3},{5,4},{6,5},{7,6},{8,15},{9,8},{10,9... | collective-permute-start | bytes 1572872 | tf_op jit(solution)/shard_map/ppermute | solution.py:28
  203.8 13.1 %collective-permute-start.9 = (bf16[128,2048]{1,0:T(8,128)(2,1)S(1)}, bf16[128,2048]{1,0:T(8,128)(2,1)S(1)}, u32[]{:S(2)}, u32[]{:S(2)}) collective-permute-start(bf16[128,2048]{1,0:T(8,128)(2,1)S(1)} %collective-permute-done.7), channel_id=1, source_target_pairs={{0,1},{1,2},{2,3},{3,4},{4,5},{5,6},{6,7},{7,0},{8,9},{9,10},{10,1... | collective-permute-start | bytes 1572872 | tf_op jit(solution)/shard_map/ppermute | solution.py:23
  203.8 13.2 %collective-permute-start.10 = (bf16[128,2048]{1,0:T(8,128)(2,1)S(1)}, bf16[128,2048]{1,0:T(8,128)(2,1)S(1)}, u32[]{:S(2)}, u32[]{:S(2)}) collective-permute-start(bf16[128,2048]{1,0:T(8,128)(2,1)S(1)} %collective-permute-done.8), channel_id=1, source_target_pairs={{0,7},{1,0},{2,1},{3,2},{4,3},{5,4},{6,5},{7,6},{8,15},{9,8},{10,9... | collective-permute-start | bytes 1572872 | tf_op jit(solution)/shard_map/ppermute | solution.py:28
  216.9 12.2 %collective-permute-start.11 = (bf16[128,2048]{1,0:T(8,128)(2,1)S(1)}, bf16[128,2048]{1,0:T(8,128)(2,1)S(1)}, u32[]{:S(2)}, u32[]{:S(2)}) collective-permute-start(bf16[128,2048]{1,0:T(8,128)(2,1)S(1)} %collective-permute-done.9), channel_id=1, source_target_pairs={{0,1},{1,2},{2,3},{3,4},{4,5},{5,6},{6,7},{7,0},{8,9},{9,10},{10,1... | collective-permute-start | bytes 1572872 | tf_op jit(solution)/shard_map/ppermute | solution.py:23
  217.1 12.2 %collective-permute-start.12 = (bf16[128,2048]{1,0:T(8,128)(2,1)S(1)}, bf16[128,2048]{1,0:T(8,128)(2,1)S(1)}, u32[]{:S(2)}, u32[]{:S(2)}) collective-permute-start(bf16[128,2048]{1,0:T(8,128)(2,1)S(1)} %collective-permute-done.10), channel_id=1, source_target_pairs={{0,7},{1,0},{2,1},{3,2},{4,3},{5,4},{6,5},{7,6},{8,15},{9,8},{10,9... | collective-permute-start | bytes 1572872 | tf_op jit(solution)/shard_map/ppermute | solution.py:28
  229.2 11.4 %collective-permute-start.13 = (bf16[128,2048]{1,0:T(8,128)(2,1)S(1)}, bf16[128,2048]{1,0:T(8,128)(2,1)S(1)}, u32[]{:S(2)}, u32[]{:S(2)}) collective-permute-start(bf16[128,2048]{1,0:T(8,128)(2,1)S(1)} %collective-permute-done.11), channel_id=1, source_target_pairs={{0,1},{1,2},{2,3},{3,4},{4,5},{5,6},{6,7},{7,0},{8,9},{9,10},{10,1... | collective-permute-start | bytes 1572872 | tf_op jit(solution)/shard_map/ppermute | solution.py:23
  240.6 2.0 copy-start.2
Sparse Core Ops, SparseCore 0:
  13.8 102.1 all-gather.1
  133.5 54.0 reduce-scatter.2
  258.7 58.8 reduce-scatter.4
